TPU v7x, 32 devices: a whole 2x2x4 slice. The times are simulated.
32 devices in a mesh: grp: 2 (over y), kv: 4 (over z), tp: 4 (over x, core).
Axes of the slice: x: 2, y: 2, z: 4, core: 2. Of those that a mesh axis runs over, the one named last changes fastest.
Arguments:
- tokens: bfloat16 [64, 4096], P('grp', ('kv', 'tp')), parts along dimension 0, may hold values from -12 to 12
- gain_in: float32 [4096], P('kv'), may hold values from 0.1 to 1.9
- w_query: bfloat16 [4096, 1024], P('kv', 'tp'), may hold values from -0.09375 to 0.09375
- w_key: bfloat16 [4096, 1024], P('kv', 'tp'), may hold values from -0.09375 to 0.09375
- w_value: bfloat16 [4096, 2048], P('kv', 'tp'), may hold values from -0.09375 to 0.09375
- w_outgate: bfloat16 [4096, 2048], P('kv', 'tp'), may hold values from -0.09375 to 0.09375
- w_input_gate: bfloat16 [4096, 16], P('kv'), may hold values from -0.09375 to 0.09375
- w_forget_gate: bfloat16 [4096, 16], P('kv'), may hold values from -0.09375 to 0.09375
- bias_input: float32 [16], replicated, may hold values from -1 to 1
- bias_forget: float32 [16], replicated, may hold values from -1 to 4
- cell_state: float32 [64, 16, 64, 128], P(('grp', 'kv'), 'tp'), parts along dimension 0, may hold values from -6 to 6
- norm_state: float32 [64, 16, 64], P(('grp', 'kv'), 'tp'), parts along dimension 0, may hold values from -18 to 18
- max_state: float32 [64, 16], P(('grp', 'kv'), 'tp'), parts along dimension 0, may hold values from -1 to 2
- w_proj: bfloat16 [2048, 4096], P('tp', 'kv'), may hold values from -0.125 to 0.125
- gain_mid: float32 [4096], P('kv'), may hold values from 0.1 to 1.9
- w_up: bfloat16 [4096, 16384], P('kv', 'tp'), may hold values from -0.09375 to 0.09375
- w_down: bfloat16 [16384, 4096], P('tp', 'kv'), may hold values from -0.046875 to 0.046875
Outputs:
- mixed: bfloat16 [64, 4096], P('grp', ('kv', 'tp')), parts along dimension 0
- cell_new: float32 [64, 16, 64, 128], P(('grp', 'kv'), 'tp'), parts along dimension 0
- norm_new: float32 [64, 16, 64], P(('grp', 'kv'), 'tp'), parts along dimension 0
- max_new: float32 [64, 16], P(('grp', 'kv'), 'tp'), parts along dimension 0
There are 2 independent parts, one for each index of `grp`. A program takes and returns all parts, laid end to end along the dimension named above; an argument that names none is the same for every part. Nothing has to cross between parts.
All inputs are finite; a program needn't handle non-finite values.
Results may differ from a plain program's by a relative error of at most 0.015.
Values may be sent and summed in bfloat16 or wider, within the bound.
A program may use at most 64 MiB of HBM per device.

v0:
```python
import functools

import jax
import jax.numpy as jnp
from jax import lax
from jax.experimental import pallas as pl
from jax.experimental.pallas import tpu as pltpu
from jax.sharding import PartitionSpec as P

MESH = pl.DeviceIdType.MESH
BF16 = jnp.bfloat16
F32 = jnp.float32

EPSILON = 1e-06


def memory_step(
    query, keys, values, outgate, log_input, log_forget, cell_state, norm_state, max_state
):
    max_new = jnp.maximum(log_forget + max_state, log_input)
    keep = jnp.exp(log_forget + max_state - max_new)
    write = jnp.exp(log_input - max_new)
    cell_new = (
        keep[..., None, None] * cell_state
        + (write[..., None] * keys)[..., :, None] * values[..., None, :]
    )
    norm_new = keep[..., None] * norm_state + write[..., None] * keys
    numer = jnp.einsum("shk,shkv->shv", query, cell_new, precision=lax.Precision.HIGHEST)
    denom = jnp.maximum(jnp.abs(jnp.sum(query * norm_new, axis=-1)), jnp.exp(-max_new))
    heads = (jax.nn.sigmoid(outgate) * numer / denom[..., None]).astype(jnp.bfloat16)
    return (heads, cell_new, norm_new, max_new)


def matmul(left, right):
    return jnp.dot(left, right, preferred_element_type=jnp.float32)


def plain_on_device(
    tokens,
    gain_in,
    w_query,
    w_key,
    w_value,
    w_outgate,
    w_input_gate,
    w_forget_gate,
    bias_input,
    bias_forget,
    cell_state,
    norm_state,
    max_state,
    w_proj,
    gain_mid,
    w_up,
    w_down,
):
    seq_local, head_count = (cell_state.shape[0], cell_state.shape[1])
    key_dim, value_dim = (cell_state.shape[2], cell_state.shape[3])
    head_start = lax.axis_index("tp") * head_count
    column_width = tokens.shape[1]
    D = gain_in.shape[0] * lax.axis_size("kv")
    gathered = lax.all_gather(tokens, "tp", axis=1, tiled=True)
    widef = gathered.astype(jnp.float32)
    part_squares = jnp.sum(widef * widef, axis=1)
    normed = (widef * gain_in).astype(jnp.bfloat16)
    gate_input = lax.dynamic_slice_in_dim(w_input_gate, head_start, head_count, 1)
    gate_forget = lax.dynamic_slice_in_dim(w_forget_gate, head_start, head_count, 1)
    terms = jnp.concatenate(
        [
            matmul(normed, w_query),
            matmul(normed, w_key),
            matmul(normed, w_value),
            matmul(normed, w_outgate),
            matmul(normed, gate_input),
            matmul(normed, gate_forget),
        ],
        axis=1,
    )
    total_squares = lax.psum(part_squares, "kv")
    own_terms = lax.psum_scatter(terms, "kv", scatter_dimension=0, tiled=True)
    row_squares = lax.dynamic_slice_in_dim(
        total_squares, lax.axis_index("kv") * seq_local, seq_local, 0
    )
    own_terms = own_terms * lax.rsqrt(row_squares / D + EPSILON)[:, None]
    width_qk = head_count * key_dim
    width_v = head_count * value_dim
    query = own_terms[:, :width_qk].reshape(seq_local, head_count, key_dim) * key_dim ** (-0.5)
    keys = own_terms[:, width_qk : 2 * width_qk].reshape(seq_local, head_count, key_dim)
    offset = 2 * width_qk
    values = own_terms[:, offset : offset + width_v].reshape(seq_local, head_count, value_dim)
    offset = offset + width_v
    outgate = own_terms[:, offset : offset + width_v].reshape(seq_local, head_count, value_dim)
    offset = offset + width_v
    log_input = own_terms[:, offset : offset + head_count] + lax.dynamic_slice_in_dim(
        bias_input, head_start, head_count, 0
    )
    offset = offset + head_count
    log_forget = jax.nn.log_sigmoid(
        own_terms[:, offset : offset + head_count]
        + lax.dynamic_slice_in_dim(bias_forget, head_start, head_count, 0)
    )
    heads, cell_new, norm_new, max_new = memory_step(
        query, keys, values, outgate, log_input, log_forget, cell_state, norm_state, max_state
    )
    branch_part = matmul(
        lax.all_gather(heads.reshape(seq_local, width_v), "kv", axis=0, tiled=True), w_proj
    )
    branch = lax.psum(branch_part, "tp")
    middle = (widef + branch).astype(jnp.bfloat16)
    midf = middle.astype(jnp.float32)
    mid_squares = jnp.sum(midf * midf, axis=1)
    normed_mid = (midf * gain_mid).astype(jnp.bfloat16)
    up_part = matmul(normed_mid, w_up)
    up_rows, square_rows = (
        lax.psum_scatter(up_part, "kv", scatter_dimension=0, tiled=True),
        lax.psum_scatter(mid_squares, "kv", scatter_dimension=0, tiled=True),
    )
    upward = up_rows * lax.rsqrt(square_rows / D + EPSILON)[:, None]
    hidden = jnp.square(jax.nn.relu(upward)).astype(jnp.bfloat16)
    down_part = matmul(lax.all_gather(hidden, "kv", axis=0, tiled=True), w_down)
    own_down = lax.psum_scatter(
        down_part.astype(jnp.bfloat16), "tp", scatter_dimension=1, tiled=True
    ).astype(jnp.float32)
    residual = lax.dynamic_slice_in_dim(midf, lax.axis_index("tp") * column_width, column_width, 1)
    mixed = (residual + own_down).astype(jnp.bfloat16)
    return (mixed, cell_new, norm_new, max_new)


def matmul_nt(left, right):
    return lax.dot_general(left, right, (((1,), (1,)), ((), ())), preferred_element_type=F32)


class Exchange:
    def __init__(self, sems):
        self.send_sem, self.recv_sem = sems
        self.used = 0
        self.started = []

    def copy(self, axis, target, src, dst, when=None):
        index = self.used
        self.used += 1
        one = pltpu.make_async_remote_copy(
            src_ref=src,
            dst_ref=dst,
            send_sem=self.send_sem.at[index],
            recv_sem=self.recv_sem.at[index],
            device_id={axis: target},
            device_id_type=MESH,
        )
        if when is None:
            one.start()
        else:
            pl.when(when)(one.start)
        self.started.append(one)
        return one


def partners(me, count):
    if count == 4:
        both = [3 - me, lax.rem(me + 2, 4), me + 1 - 2 * lax.rem(me, 2)]
        return both, both
    ahead = [lax.rem(me + o, count) for o in range(1, count)]
    behind = [lax.rem(me + count - o, count) for o in range(1, count)]
    return ahead, behind


def count_copies(kv, tp, subs):
    return 3 * (tp - 1) + 5 * (kv - 1) + 2 * subs * (kv - 1)


def layer_kernel(
    kv,
    tp,
    subs,
    tokens,
    gain_in,
    w_query,
    w_key,
    w_value,
    w_outgate,
    w_input_gate,
    w_forget_gate,
    bias_input,
    bias_forget,
    cell_state,
    norm_state,
    max_state,
    w_proj,
    gain_mid,
    w_up,
    w_down,
    out_v,
    cell_o,
    norm_o,
    max_o,
    tok,
    gain1,
    wqkv,
    wgi,
    wgf,
    bi,
    bf,
    cell,
    norm,
    mstate,
    wproj,
    gain2,
    wup,
    wdown,
    terms,
    b_send,
    b_recv,
    g_send,
    g_recv,
    numer,
    h_all,
    e_all,
    sq_all,
    mid,
    nmid,
    f_own,
    f_send,
    f_recv,
    hid,
    down,
    d_send,
    d_recv,
    in_sem,
    send_sem,
    recv_sem,
):
    k_me, t_me = lax.axis_index("kv"), lax.axis_index("tp")
    link = Exchange((send_sem, recv_sem))
    rows, width = tok.shape[1], tok.shape[2]
    own_rows, n_heads, key_dim, value_dim = cell.shape
    wide = tp * width
    total_width = kv * wide
    w_qk, w_v = n_heads * key_dim, n_heads * value_dim
    half = f_own.shape[2]
    block = subs * half

    loads = []

    def load(src, dst):
        one = pltpu.make_async_copy(src, dst, in_sem.at[len(loads)])
        one.start()
        loads.append(one)
        return one

    l_tok = load(tokens, tok.at[t_me])
    l_gain = load(gain_in, gain1)
    l_q = load(w_query, wqkv.at[:, 0:w_qk])
    l_k = load(w_key, wqkv.at[:, w_qk : 2 * w_qk])
    l_v = load(w_value, wqkv.at[:, 2 * w_qk : 2 * w_qk + w_v])
    l_o = load(w_outgate, wqkv.at[:, 2 * w_qk + w_v : 2 * w_qk + 2 * w_v])
    l_gates = [load(w_input_gate, wgi), load(w_forget_gate, wgf)]
    l_small = [
        load(bias_input, bi),
        load(bias_forget, bf),
        load(norm_state, norm),
        load(max_state, mstate),
    ]

    barrier = pltpu.get_barrier_semaphore()
    k_peers, k_from = partners(k_me, kv)
    t_peers, t_from = partners(t_me, tp)
    for peer in t_peers:
        pl.semaphore_signal(barrier, inc=1, device_id={"tp": peer}, device_id_type=MESH)
    for peer in k_peers:
        pl.semaphore_signal(barrier, inc=1, device_id={"kv": peer}, device_id_type=MESH)
    g_send[...] = jnp.zeros_like(g_send)
    l_tok.wait()
    pl.semaphore_wait(barrier, kv + tp - 2)

    a_copies = [link.copy("tp", p, tok.at[t_me], tok.at[t_me]) for p in t_peers]
    l_cell = load(cell_state, cell)
    l_proj = load(w_proj, wproj)
    l_gain2 = load(gain_mid, gain2)
    l_up = load(w_up, wup)
    l_down = [
        load(w_down.at[pl.ds(i * block, block)], wdown.at[pl.ds(i * block, block)])
        for i in range(kv)
    ]
    l_gain.wait()
    for one in a_copies:
        one.wait_recv()
    wide_f = jnp.concatenate([tok[i] for i in range(tp)], axis=1).astype(F32)
    squares = jnp.sum(wide_f * wide_f, axis=1, keepdims=True)
    normed = (wide_f * gain1[...]).astype(BF16)

    for one in l_gates:
        one.wait()
    n_gates = wgi.shape[0]
    shape_g = (kv, own_rows, n_gates)
    g_send[:, :, 0:n_gates] = matmul_nt(normed, wgi[...]).reshape(shape_g)
    g_send[:, :, 128 : 128 + n_gates] = matmul_nt(normed, wgf[...]).reshape(shape_g)
    g_send[:, :, 256:384] = jnp.broadcast_to(squares, (rows, 128)).reshape(kv, own_rows, 128)
    g_copies = [
        link.copy("kv", p, g_send.at[p], g_recv.at[o]) for o, p in enumerate(k_peers)
    ]
    for one in (l_q, l_k, l_v, l_o):
        one.wait()
    tile = 256

    def project(i, carry):
        cols = pl.ds(pl.multiple_of(i * tile, tile), tile)
        part = matmul(normed, wqkv[:, cols]).reshape(kv, own_rows, tile)
        terms[:, :, cols] = part
        b_send[:, :, cols] = part.astype(BF16)
        return carry

    n_tiles = wqkv.shape[1] // tile
    b_copies = []
    for low, high in ((0, n_tiles // 2), (n_tiles // 2, n_tiles)):
        lax.fori_loop(low, high, project, 0)
        cols = pl.ds(low * tile, (high - low) * tile)
        for o, p in enumerate(k_peers):
            here = b_send.at[p, :, cols], b_recv.at[o, :, cols]
            b_copies.append(link.copy("kv", p, *here))

    for one in l_small:
        one.wait()
    l_cell.wait()
    for one in g_copies:
        one.wait_recv()
    gates = g_send[k_me]
    for o in range(kv - 1):
        gates = gates + g_recv[o]
    scale = lax.rsqrt(gates[:, 256:257] / total_width + EPSILON)
    log_i = gates[:, 0:n_gates] * scale + bi[...]
    raw_f = gates[:, 128 : 128 + n_gates] * scale + bf[...]
    log_f = jnp.minimum(raw_f, 0.0) - jnp.log1p(jnp.exp(-jnp.abs(raw_f)))
    gate_lane = lax.broadcasted_iota(jnp.int32, (own_rows, n_gates), 1)
    keep, write, floor = [], [], []
    max_cols = []
    old_max = mstate[...].T
    for h in range(n_heads):
        pick = gate_lane == t_me * n_heads + h
        li = jnp.sum(jnp.where(pick, log_i, 0.0), axis=1, keepdims=True)
        lf = jnp.sum(jnp.where(pick, log_f, 0.0), axis=1, keepdims=True)
        old = old_max[:, h : h + 1]
        new = jnp.maximum(lf + old, li)
        max_cols.append(new)
        keep.append(jnp.exp(lf + old - new))
        write.append(jnp.exp(li - new))
        floor.append(jnp.exp(-new))
    head_lane = lax.broadcasted_iota(jnp.int32, (own_rows, n_heads), 1)
    new_max = jnp.broadcast_to(max_cols[0], (own_rows, n_heads))
    for h in range(1, n_heads):
        new_max = jnp.where(head_lane == h, max_cols[h], new_max)
    max_o[...] = new_max.T
    for one in b_copies:
        one.wait_recv()
    own = terms[k_me]
    for o in range(kv - 1):
        own = own + b_recv[o].astype(F32)
    own = own * scale
    query = own[:, 0:w_qk] * key_dim ** (-0.5)
    keys = own[:, w_qk : 2 * w_qk]
    values = own[:, 2 * w_qk : 2 * w_qk + w_v]
    outgate = own[:, 2 * w_qk + w_v : 2 * w_qk + 2 * w_v]
    qk_head = lax.broadcasted_iota(jnp.int32, (own_rows, w_qk), 1) // key_dim
    spread = jnp.broadcast_to(write[0], (own_rows, w_qk))
    for h in range(1, n_heads):
        spread = jnp.where(qk_head == h, write[h], spread)
    wkeys = keys * spread
    pad = jnp.zeros((128 - 2 * own_rows, w_qk), F32)
    turned = jnp.concatenate([wkeys, query, pad], axis=0).T
    denom, cross = [], []
    for h in range(n_heads):
        part = slice(h * key_dim, (h + 1) * key_dim)
        fresh = keep[h] * norm[:, h, :] + wkeys[:, part]
        norm_o[:, h, :] = fresh
        dot = jnp.sum(query[:, part] * fresh, axis=1, keepdims=True)
        shape_v = (own_rows, value_dim)
        denom.append(jnp.broadcast_to(jnp.maximum(jnp.abs(dot), floor[h]), shape_v))
        dot = jnp.sum(query[:, part] * wkeys[:, part], axis=1, keepdims=True)
        cross.append(jnp.broadcast_to(dot, shape_v))
    for h in range(n_heads):
        part = slice(h * key_dim, (h + 1) * key_dim)
        vals = slice(h * value_dim, (h + 1) * value_dim)
        for s in range(own_rows):
            q_col = turned[part, own_rows + s : own_rows + s + 1]
            numer[s : s + 1, vals] = jnp.sum(q_col * cell[s, h], axis=0, keepdims=True)
    keep_v = jnp.concatenate(
        [jnp.broadcast_to(one, (own_rows, value_dim)) for one in keep], axis=1
    )
    above = keep_v * numer[...] + jnp.concatenate(cross, axis=1) * values
    heads = jax.nn.sigmoid(outgate) * above / jnp.concatenate(denom, axis=1)
    h_all[k_me] = heads.astype(BF16)
    h_copies = [link.copy("kv", p, h_all.at[k_me], h_all.at[k_me]) for p in k_peers]
    for h in range(n_heads):
        part = slice(h * key_dim, (h + 1) * key_dim)
        vals = slice(h * value_dim, (h + 1) * value_dim)
        for s in range(own_rows):
            cell_o[s, h] = (
                keep[h][s : s + 1, :] * cell[s, h]
                + turned[part, s : s + 1] * values[s : s + 1, vals]
            )
    l_proj.wait()
    for one in h_copies:
        one.wait_recv()
    all_heads = jnp.concatenate([h_all[i].astype(F32) for i in range(kv)], axis=0)

    e_all[t_me] = matmul(all_heads.astype(BF16), wproj[...]).astype(BF16)
    e_copies = [link.copy("tp", p, e_all.at[t_me], e_all.at[t_me]) for p in t_peers]
    l_gain2.wait()
    for one in e_copies:
        one.wait_recv()
    branch = e_all[0].astype(F32)
    for i in range(1, tp):
        branch = branch + e_all[i].astype(F32)
    wide_f = jnp.concatenate([tok[i] for i in range(tp)], axis=1).astype(F32)
    middle = (wide_f + branch).astype(BF16).astype(F32)
    for i in range(tp):
        mid[i] = middle[:, i * width : (i + 1) * width]
    sq_all[k_me] = jnp.broadcast_to(jnp.sum(middle * middle, axis=1, keepdims=True), (rows, 128))
    s_copies = [link.copy("kv", p, sq_all.at[k_me], sq_all.at[k_me]) for p in k_peers]
    nmid[...] = (middle * gain2[...]).astype(BF16)

    l_up.wait()
    f_copies = {}

    def raise_block(target, sub, put):
        first = target * block + sub * half

        def raise_tile(i, carry):
            cols = pl.ds(pl.multiple_of(first + i * tile, tile), tile)
            put(pl.ds(pl.multiple_of(i * tile, tile), tile), matmul(nmid[...], wup[:, cols]))
            return carry

        lax.fori_loop(0, half // tile, raise_tile, 0)

    is_end = jnp.logical_or(k_me == 0, k_me == kv - 1)
    is_mid = jnp.logical_not(is_end)
    across, skip, near = k_peers
    targets = [across, jnp.where(is_end, near, skip), near]
    for o in (1, 0, 2):
        for sub in range(subs):

            def put_sent(here, part, o=o, sub=sub):
                f_send[o, sub, :, here] = part.astype(BF16)

            raise_block(k_peers[o], sub, put_sent)
            f_copies[o, sub] = link.copy(
                "kv",
                targets[o],
                f_send.at[o, sub],
                f_recv.at[o, sub],
                when=None if o else is_end,
            )
    for sub in range(subs):
        f_copies[1, sub].wait_recv()

        def relay(sub=sub):
            both = f_send[0, sub].astype(F32) + f_recv[1, sub].astype(F32)
            f_send[0, sub] = both.astype(BF16)
            f_copies[0, sub].start()

        pl.when(is_mid)(relay)

        def put_own(here, part, sub=sub):
            f_own[sub, :, here] = part

        raise_block(k_me, sub, put_own)
    for one in s_copies:
        one.wait_recv()
    row_sum = sq_all[0, :, 0:1]
    for i in range(1, kv):
        row_sum = row_sum + sq_all[i, :, 0:1]
    scale_mid = lax.rsqrt(row_sum / total_width + EPSILON)
    g2_copies = {}
    for sub in range(subs):
        upward = f_own[sub]
        f_copies[0, sub].wait_recv()
        f_copies[2, sub].wait_recv()
        skipped = jnp.where(is_end, f_recv[1, sub].astype(F32), 0.0)
        upward = upward + f_recv[0, sub].astype(F32) + skipped + f_recv[2, sub].astype(F32)
        hid[k_me, sub] = jnp.square(jnp.maximum(upward * scale_mid, 0.0)).astype(BF16)
        mine = hid.at[k_me, sub]
        for o, peer in enumerate(k_peers):
            g2_copies[o, sub] = link.copy("kv", peer, mine, mine)

    for one in l_down:
        one.wait()

    def lower_block(source, sub, first):
        deep = pl.ds(pl.multiple_of(source * block + sub * half, half), half)
        part = matmul(hid[source, sub], wdown[deep, :])
        down[...] = part if first else down[...] + part

    for sub in range(subs):
        lower_block(k_me, sub, sub == 0)
    for sub in range(subs):
        for o in (2, 1, 0):
            g2_copies[o, sub].wait_recv()
            lower_block(k_from[o], sub, False)
    for i in range(tp):
        d_send[i] = down[:, i * width : (i + 1) * width].astype(BF16)
    d_copies = [
        link.copy("tp", p, d_send.at[p], d_recv.at[o]) for o, p in enumerate(t_peers)
    ]
    lower = d_send[t_me].astype(F32)
    for o, one in enumerate(d_copies):
        one.wait_recv()
        lower = lower + d_recv[o].astype(F32)
    out_v[...] = (mid[t_me] + lower).astype(BF16)
    for one in link.started:
        one.wait_send()


def finish_kernel(*refs):
    sources, outs, sem = refs[0:4], refs[4:8], refs[8]
    copies = [pltpu.make_async_copy(sources[i], outs[i], sem.at[i]) for i in range(4)]
    for one in copies:
        one.start()
    for one in copies:
        one.wait()


def fused_on_device(kv, tp, *args):
    (tokens, gain_in, w_query, w_key, w_value, w_outgate, w_input_gate, w_forget_gate) = args[:8]
    (bias_input, bias_forget, cell_state, norm_state, max_state) = args[8:13]
    (w_proj, gain_mid, w_up, w_down) = args[13:]
    rows, width = tokens.shape
    own_rows = cell_state.shape[0]
    wide = w_query.shape[0]
    n_qkv = w_query.shape[1] + w_key.shape[1] + w_value.shape[1] + w_outgate.shape[1]
    hidden = w_up.shape[1]
    subs = 4 if hidden % (1024 * kv) == 0 else 2
    half = hidden // (kv * subs)
    w_v = w_value.shape[1]
    operands = tuple(pltpu.with_memory_space_constraint(x, pltpu.HBM) for x in (
        tokens,
        gain_in.reshape(1, -1),
        w_query,
        w_key,
        w_value,
        w_outgate,
        w_input_gate.T,
        w_forget_gate.T,
        bias_input.reshape(1, -1),
        bias_forget.reshape(1, -1),
        cell_state,
        norm_state,
        max_state.T,
        w_proj,
        gain_mid.reshape(1, -1),
        w_up,
        w_down,
    ))
    n_copies = count_copies(kv, tp, subs)
    vm = pltpu.VMEM
    scratch = [
        vm((tp, rows, width), BF16),
        vm((1, wide), F32),
        vm((wide, n_qkv), BF16),
        vm(w_input_gate.shape[::-1], BF16),
        vm(w_forget_gate.shape[::-1], BF16),
        vm((1, bias_input.shape[0]), F32),
        vm((1, bias_forget.shape[0]), F32),
        vm(cell_state.shape, F32),
        vm(norm_state.shape, F32),
        vm(max_state.shape[::-1], F32),
        vm(w_proj.shape, BF16),
        vm((1, wide), F32),
        vm(w_up.shape, BF16),
        vm(w_down.shape, BF16),
        vm((kv, own_rows, n_qkv), F32),
        vm((kv, own_rows, n_qkv), BF16),
        vm((kv - 1, own_rows, n_qkv), BF16),
        vm((kv, own_rows, 384), F32),
        vm((kv - 1, own_rows, 384), F32),
        vm((own_rows, w_v), F32),
        vm((kv, own_rows, w_v), BF16),
        vm((tp, rows, wide), BF16),
        vm((kv, rows, 128), F32),
        vm((tp, rows, width), F32),
        vm((rows, wide), BF16),
        vm((subs, rows, half), F32),
        vm((kv - 1, subs, rows, half), BF16),
        vm((kv - 1, subs, rows, half), BF16),
        vm((kv, subs, rows, half), BF16),
        vm((rows, wide), F32),
        vm((tp, rows, width), BF16),
        vm((tp - 1, rows, width), BF16),
        pltpu.SemaphoreType.DMA((16 + kv,)),
        pltpu.SemaphoreType.DMA((n_copies,)),
        pltpu.SemaphoreType.DMA((n_copies,)),
    ]
    anywhere = pl.BlockSpec(memory_space=pltpu.HBM)
    in_vmem = pl.BlockSpec(memory_space=pltpu.VMEM)
    results = pl.pallas_call(
        functools.partial(layer_kernel, kv, tp, subs),
        out_shape=(
            jax.ShapeDtypeStruct((rows, width), BF16),
            jax.ShapeDtypeStruct(cell_state.shape, F32),
            jax.ShapeDtypeStruct(norm_state.shape, F32),
            jax.ShapeDtypeStruct(max_state.shape[::-1], F32),
        ),
        in_specs=[anywhere] * len(operands),
        out_specs=(in_vmem,) * 4,
        scratch_shapes=scratch,
        compiler_params=pltpu.CompilerParams(
            collective_id=0, has_side_effects=True, vmem_limit_bytes=36 * 1024 * 1024
        ),
    )(*operands)
    mixed, cell_new, norm_new, max_new = pl.pallas_call(
        finish_kernel,
        out_shape=tuple(jax.ShapeDtypeStruct(one.shape, one.dtype) for one in results),
        in_specs=[in_vmem] * 4,
        out_specs=(anywhere,) * 4,
        scratch_shapes=[pltpu.SemaphoreType.DMA((4,))],
        compiler_params=pltpu.CompilerParams(vmem_limit_bytes=8 * 1024 * 1024),
    )(*results)
    return (mixed, cell_new, norm_new, max_new.T)


def fits_kernel(kv, tp, *args):
    tokens, w_query, cell_state, w_up = args[0], args[2], args[10], args[15]
    return (
        kv == 4
        and tp > 1
        and tokens.shape[1] % 128 == 0
        and w_query.shape[0] % 256 == 0
        and w_query.shape[1] % 256 == 0
        and args[4].shape[1] % 256 == 0
        and cell_state.shape[0] % 8 == 0
        and 2 * cell_state.shape[0] <= 128
        and cell_state.shape[3] % 128 == 0
        and w_up.shape[1] % (512 * kv) == 0
        and args[6].shape[1] <= 128
    )


def on_device(kv, tp, *args):
    if fits_kernel(kv, tp, *args):
        return fused_on_device(kv, tp, *args)
    return plain_on_device(*args)


def solution(mesh):
    in_specs = (
        P("grp", ("kv", "tp")),
        P("kv"),
        P("kv", "tp"),
        P("kv", "tp"),
        P("kv", "tp"),
        P("kv", "tp"),
        P("kv", None),
        P("kv", None),
        P(),
        P(),
        P(("grp", "kv"), "tp", None, None),
        P(("grp", "kv"), "tp", None),
        P(("grp", "kv"), "tp"),
        P("tp", "kv"),
        P("kv"),
        P("kv", "tp"),
        P("tp", "kv"),
    )
    out_specs = (
        P("grp", ("kv", "tp")),
        P(("grp", "kv"), "tp", None, None),
        P(("grp", "kv"), "tp", None),
        P(("grp", "kv"), "tp"),
    )
    return jax.shard_map(
        functools.partial(on_device, mesh.shape["kv"], mesh.shape["tp"]),
        mesh=mesh, in_specs=in_specs, out_specs=out_specs, check_vma=False
    )
```

profile of v0, /device:TPU:0, one launch (start us, length us, event | category | flops | bytes accessed | tf_op | source)
XLA Modules:
  0.0 41.4 jit_solution(11197015269140442434)
XLA Ops:
  0.6 39.7 %shard_map.192 = (bf16[32,256]{1,0:T(8,128)(2,1)S(1)}, f32[8,4,64,128]{3,2,1,0:T(8,128)S(1)}, f32[8,4,64]{2,1,0:T(4,128)S(1)}, f32[4,8]{1,0:T(4,128)S(1)}) custom-call(bf16[32,256]{1,0:T(8,128)(2,1)} %tokens.1, f32[1,1024]{1,0:T(1,128)} %bitcast.10, bf16[1024,256]{1,0:T(8,128)(2,1)} %w_query.1, bf16[1024,256]{1,0:T(8,128)(2,1)} %w_key.1, ...), custom_call_target="tpu_custom_call" | custom-call | tf_op jit(solution)/shard_map/pallas_call | solution.py:593
  40.4 1.0 %shard_map.193 = (bf16[32,256]{1,0:T(8,128)(2,1)}, f32[8,4,64,128]{3,2,1,0:T(8,128)}, f32[8,4,64]{2,1,0:T(4,128)}, f32[4,8]{1,0:T(4,128)}) custom-call(bf16[32,256]{1,0:T(8,128)(2,1)S(1)} %get-tuple-element.12.refs_0_, f32[8,4,64,128]{3,2,1,0:T(8,128)S(1)} %get-tuple-element.13.refs_1_, f32[8,4,64]{2,1,0:T(4,128)S(1)} %get-tuple-element.14.refs_2_, ...), custom_call_target="tpu_custom_call" | custom-call | tf_op jit(solution)/shard_map/pallas_call | solution.py:608
where the time goes:
time: 41.6 us; the launch traced here: 41.4 us
  Pallas kernels  40.7 us (98%)
  between operations  0.65 us (2%)
    pallas_call x1, Pallas kernels, fused_on_device(): pl.pallas_call(functools.partial(layer_kernel, kv, tp, subs), out_shape=(...  39.7 us
    pallas_call x1, Pallas kernels, fused_on_device(): pl.pallas_call(finish_kernel, out_shape=tuple((jax.ShapeDtypeStruct(one.s...  1.02 us

commit v1 on v0

--- a/solution.py
+++ b/solution.py
@@ -130,42 +130,40 @@
     return lax.dot_general(left, right, (((1,), (1,)), ((), ())), preferred_element_type=F32)
 
 
-class Exchange:
-    def __init__(self, sems):
-        self.send_sem, self.recv_sem = sems
-        self.used = 0
-        self.started = []
-
-    def copy(self, axis, target, src, dst, when=None):
+def partners(me, count):
+    both = [3 - me, lax.rem(me + 2, 4), me + 1 - 2 * lax.rem(me, 2)]
+    return both, both
+
+
+class Link:
+    def __init__(self, send_sem, recv_sem):
+        self.send_sem, self.recv_sem = send_sem, recv_sem
+        self.sent, self.used = 0, 0
+
+    def phase(self):
+        index = self.sent
+        self.sent += 1
+        return self.send_sem.at[index]
+
+    def slot(self):
         index = self.used
         self.used += 1
-        one = pltpu.make_async_remote_copy(
-            src_ref=src,
-            dst_ref=dst,
-            send_sem=self.send_sem.at[index],
-            recv_sem=self.recv_sem.at[index],
-            device_id={axis: target},
-            device_id_type=MESH,
-        )
-        if when is None:
-            one.start()
-        else:
-            pl.when(when)(one.start)
-        self.started.append(one)
-        return one
-
-
-def partners(me, count):
-    if count == 4:
-        both = [3 - me, lax.rem(me + 2, 4), me + 1 - 2 * lax.rem(me, 2)]
-        return both, both
-    ahead = [lax.rem(me + o, count) for o in range(1, count)]
-    behind = [lax.rem(me + count - o, count) for o in range(1, count)]
-    return ahead, behind
-
-
-def count_copies(kv, tp, subs):
-    return 3 * (tp - 1) + 5 * (kv - 1) + 2 * subs * (kv - 1)
+        return self.recv_sem.at[index]
+
+
+def remote(src, dst, send, recv, where):
+    return pltpu.make_async_remote_copy(
+        src_ref=src,
+        dst_ref=dst,
+        send_sem=send,
+        recv_sem=recv,
+        device_id=where,
+        device_id_type=MESH,
+    )
+
+
+def semaphore_counts(subs):
+    return 12, 10, 10 + 3 * subs
 
 
 def layer_kernel(
@@ -196,10 +194,8 @@
     tok,
     gain1,
     wqkv,
-    wgi,
-    wgf,
-    bi,
-    bf,
+    wg,
+    bias,
     cell,
     norm,
     mstate,
@@ -230,105 +226,136 @@
     recv_sem,
 ):
     k_me, t_me = lax.axis_index("kv"), lax.axis_index("tp")
-    link = Exchange((send_sem, recv_sem))
+    core = lax.rem(t_me, 2)
+    mate = t_me + 1 - 2 * core
+    link = Link(send_sem, recv_sem)
     rows, width = tok.shape[1], tok.shape[2]
     own_rows, n_heads, key_dim, value_dim = cell.shape
     wide = tp * width
     total_width = kv * wide
     w_qk, w_v = n_heads * key_dim, n_heads * value_dim
+    n_gates = bias.shape[2]
     half = f_own.shape[2]
     block = subs * half
-
-    loads = []
-
-    def load(src, dst):
-        one = pltpu.make_async_copy(src, dst, in_sem.at[len(loads)])
-        one.start()
-        loads.append(one)
-        return one
-
-    l_tok = load(tokens, tok.at[t_me])
-    l_gain = load(gain_in, gain1)
-    l_q = load(w_query, wqkv.at[:, 0:w_qk])
-    l_k = load(w_key, wqkv.at[:, w_qk : 2 * w_qk])
-    l_v = load(w_value, wqkv.at[:, 2 * w_qk : 2 * w_qk + w_v])
-    l_o = load(w_outgate, wqkv.at[:, 2 * w_qk + w_v : 2 * w_qk + 2 * w_v])
-    l_gates = [load(w_input_gate, wgi), load(w_forget_gate, wgf)]
-    l_small = [
-        load(bias_input, bi),
-        load(bias_forget, bf),
-        load(norm_state, norm),
-        load(max_state, mstate),
-    ]
+    half_wide = wide // 2
+
+    groups = [0]
+
+    def load(*pairs):
+        sem = in_sem.at[groups[0]]
+        groups[0] += 1
+        for src, dst in pairs:
+            pltpu.make_async_copy(src, dst, sem).start()
+        return sem
+
+    def loaded(sem, whole):
+        pltpu.make_async_copy(whole, whole, sem).wait()
+
+    def columns(first, size):
+        return pl.ds(pl.multiple_of(first, size), size)
+
+    l_tok = load((tokens, tok.at[t_me]))
+    l_gain = load((gain_in, gain1))
+    l_gates = load((w_input_gate, wg.at[0:n_gates]), (w_forget_gate, wg.at[n_gates : 2 * n_gates]))
+    l_qkv = load(
+        (w_query, wqkv.at[:, 0:w_qk]),
+        (w_key, wqkv.at[:, w_qk : 2 * w_qk]),
+        (w_value, wqkv.at[:, 2 * w_qk : 2 * w_qk + w_v]),
+        (w_outgate, wqkv.at[:, 2 * w_qk + w_v : 2 * w_qk + 2 * w_v]),
+    )
+    l_bias = load((bias_input, bias.at[0]), (bias_forget, bias.at[1]))
+    l_norm = load((norm_state, norm))
+    l_max = load((max_state, mstate))
 
     barrier = pltpu.get_barrier_semaphore()
     k_peers, k_from = partners(k_me, kv)
-    t_peers, t_from = partners(t_me, tp)
-    for peer in t_peers:
-        pl.semaphore_signal(barrier, inc=1, device_id={"tp": peer}, device_id_type=MESH)
-    for peer in k_peers:
-        pl.semaphore_signal(barrier, inc=1, device_id={"kv": peer}, device_id_type=MESH)
-    g_send[...] = jnp.zeros_like(g_send)
-    l_tok.wait()
-    pl.semaphore_wait(barrier, kv + tp - 2)
-
-    a_copies = [link.copy("tp", p, tok.at[t_me], tok.at[t_me]) for p in t_peers]
-    l_cell = load(cell_state, cell)
-    l_proj = load(w_proj, wproj)
-    l_gain2 = load(gain_mid, gain2)
-    l_up = load(w_up, wup)
-    l_down = [
-        load(w_down.at[pl.ds(i * block, block)], wdown.at[pl.ds(i * block, block)])
-        for i in range(kv)
-    ]
-    l_gain.wait()
-    for one in a_copies:
-        one.wait_recv()
-    wide_f = jnp.concatenate([tok[i] for i in range(tp)], axis=1).astype(F32)
-    squares = jnp.sum(wide_f * wide_f, axis=1, keepdims=True)
-    normed = (wide_f * gain1[...]).astype(BF16)
-
-    for one in l_gates:
-        one.wait()
-    n_gates = wgi.shape[0]
-    shape_g = (kv, own_rows, n_gates)
-    g_send[:, :, 0:n_gates] = matmul_nt(normed, wgi[...]).reshape(shape_g)
-    g_send[:, :, 128 : 128 + n_gates] = matmul_nt(normed, wgf[...]).reshape(shape_g)
-    g_send[:, :, 256:384] = jnp.broadcast_to(squares, (rows, 128)).reshape(kv, own_rows, 128)
-    g_copies = [
-        link.copy("kv", p, g_send.at[p], g_recv.at[o]) for o, p in enumerate(k_peers)
-    ]
-    for one in (l_q, l_k, l_v, l_o):
-        one.wait()
-    tile = 256
-
-    def project(i, carry):
-        cols = pl.ds(pl.multiple_of(i * tile, tile), tile)
-        part = matmul(normed, wqkv[:, cols]).reshape(kv, own_rows, tile)
+    t_far = [3 - t_me, lax.rem(t_me + 2, tp)]
+    t_peers = t_far + [mate]
+    everyone = [{"tp": p} for p in t_peers] + [{"kv": p} for p in k_peers]
+    everyone += [{"kv": p, "tp": mate} for p in k_peers]
+    for where in everyone:
+        pl.semaphore_signal(barrier, inc=1, device_id=where, device_id_type=MESH)
+    loaded(l_tok, tok.at[t_me])
+    pl.semaphore_wait(barrier, len(everyone))
+
+    a_sent, a_far, a_mate = link.phase(), link.slot(), link.slot()
+    for p in t_far:
+        remote(tok.at[t_me], tok.at[t_me], a_sent, a_far, {"tp": p}).start()
+    remote(tok.at[t_me], tok.at[t_me], a_sent, a_mate, {"tp": mate}).start()
+    w_sent, w_got = link.phase(), link.slot()
+    proj_rows = wproj.at[columns(core * w_v, w_v)]
+    remote(
+        w_proj.at[:, columns((1 - core) * half_wide, half_wide)],
+        proj_rows,
+        w_sent,
+        w_got,
+        {"tp": mate},
+    ).start()
+    l_cell = load((cell_state, cell))
+    l_proj = load((w_proj.at[:, columns(core * half_wide, half_wide)], proj_rows))
+    l_gain2 = load((gain_mid, gain2))
+    spans = [pl.ds(i * (wup.shape[0] // kv), wup.shape[0] // kv) for i in range(kv)]
+    l_up = load(*[(w_up.at[s], wup.at[s]) for s in spans])
+    spans = [pl.ds(i * block, block) for i in range(kv)]
+    l_down = load(*[(w_down.at[s], wdown.at[s]) for s in spans])
+    loaded(l_gain, gain1)
+    loaded(l_gates, wg)
+    loaded(l_qkv, wqkv)
+
+    def normed_tile(t):
+        here = columns(t * width, width)
+        tile = tok[t].astype(F32)
+        squares = jnp.sum(tile * tile, axis=1, keepdims=True)
+        tile = (tile * gain1[:, here]).astype(BF16)
+        return tile, squares, matmul_nt(tile, wg[:, here]), here
+
+    n_qkv = wqkv.shape[1]
+    flat = (kv, own_rows, n_qkv)
+    tile, squares, gate_sum, here = normed_tile(t_me)
+    terms[...] = matmul(tile, wqkv[here, :]).reshape(flat)
+    remote(tok.at[0], tok.at[0], a_sent, a_mate, {"tp": mate}).wait_recv()
+    tile, more, gate_more, here = normed_tile(mate)
+    squares, gate_sum = squares + more, gate_sum + gate_more
+    terms[...] = terms[...] + matmul(tile, wqkv[here, :]).reshape(flat)
+    remote(tok.at[0:2], tok.at[0:2], a_sent, a_far, {"tp": mate}).wait_recv()
+    far = [normed_tile(t) for t in t_far]
+    for _, more, gate_more, _ in far:
+        squares, gate_sum = squares + more, gate_sum + gate_more
+    packed = jnp.concatenate(
+        [gate_sum, jnp.broadcast_to(squares, (rows, 128 - 2 * n_gates))], axis=1
+    )
+    g_send[...] = packed.reshape(kv, own_rows, 128)
+    g_sent, g_got = link.phase(), link.slot()
+    for o, p in enumerate(k_peers):
+        remote(g_send.at[p], g_recv.at[o], g_sent, g_got, {"kv": p}).start()
+    b_sent, b_got = link.phase(), []
+    pieces = (slice(0, n_qkv // 2), slice(n_qkv // 2, n_qkv))
+    for cols in pieces:
+        size = cols.stop - cols.start
+        part = terms[:, :, cols]
+        for tile, _, _, here in far:
+            part = part + matmul(tile, wqkv[here, cols]).reshape(kv, own_rows, size)
         terms[:, :, cols] = part
         b_send[:, :, cols] = part.astype(BF16)
-        return carry
-
-    n_tiles = wqkv.shape[1] // tile
-    b_copies = []
-    for low, high in ((0, n_tiles // 2), (n_tiles // 2, n_tiles)):
-        lax.fori_loop(low, high, project, 0)
-        cols = pl.ds(low * tile, (high - low) * tile)
+        got = link.slot()
+        b_got.append(got)
         for o, p in enumerate(k_peers):
-            here = b_send.at[p, :, cols], b_recv.at[o, :, cols]
-            b_copies.append(link.copy("kv", p, *here))
-
-    for one in l_small:
-        one.wait()
-    l_cell.wait()
-    for one in g_copies:
-        one.wait_recv()
+            remote(
+                b_send.at[p, :, cols], b_recv.at[o, :, cols], b_sent, got, {"kv": p}
+            ).start()
+
+    loaded(l_bias, bias)
+    loaded(l_norm, norm)
+    loaded(l_max, mstate)
+    loaded(l_cell, cell)
+    near_kv = {"kv": k_peers[2]}
+    remote(g_recv, g_recv, g_sent, g_got, near_kv).wait_recv()
     gates = g_send[k_me]
     for o in range(kv - 1):
         gates = gates + g_recv[o]
-    scale = lax.rsqrt(gates[:, 256:257] / total_width + EPSILON)
-    log_i = gates[:, 0:n_gates] * scale + bi[...]
-    raw_f = gates[:, 128 : 128 + n_gates] * scale + bf[...]
+    scale = lax.rsqrt(gates[:, 2 * n_gates : 2 * n_gates + 1] / total_width + EPSILON)
+    log_i = gates[:, 0:n_gates] * scale + bias[0]
+    raw_f = gates[:, n_gates : 2 * n_gates] * scale + bias[1]
     log_f = jnp.minimum(raw_f, 0.0) - jnp.log1p(jnp.exp(-jnp.abs(raw_f)))
     gate_lane = lax.broadcasted_iota(jnp.int32, (own_rows, n_gates), 1)
     keep, write, floor = [], [], []
@@ -349,8 +376,9 @@
     for h in range(1, n_heads):
         new_max = jnp.where(head_lane == h, max_cols[h], new_max)
     max_o[...] = new_max.T
-    for one in b_copies:
-        one.wait_recv()
+    for cols, got in zip(pieces, b_got):
+        here = b_recv.at[:, :, cols]
+        remote(here, here, b_sent, got, near_kv).wait_recv()
     own = terms[k_me]
     for o in range(kv - 1):
         own = own + b_recv[o].astype(F32)
@@ -387,8 +415,12 @@
     )
     above = keep_v * numer[...] + jnp.concatenate(cross, axis=1) * values
     heads = jax.nn.sigmoid(outgate) * above / jnp.concatenate(denom, axis=1)
-    h_all[k_me] = heads.astype(BF16)
-    h_copies = [link.copy("kv", p, h_all.at[k_me], h_all.at[k_me]) for p in k_peers]
+    mine = core * kv + k_me
+    h_all[mine] = heads.astype(BF16)
+    h_sent, h_got = link.phase(), link.slot()
+    targets = [{"kv": p, "tp": t} for p in k_peers for t in (mate, t_me)] + [{"tp": mate}]
+    for where in targets:
+        remote(h_all.at[mine], h_all.at[mine], h_sent, h_got, where).start()
     for h in range(n_heads):
         part = slice(h * key_dim, (h + 1) * key_dim)
         vals = slice(h * value_dim, (h + 1) * value_dim)
@@ -397,116 +429,153 @@
                 keep[h][s : s + 1, :] * cell[s, h]
                 + turned[part, s : s + 1] * values[s : s + 1, vals]
             )
-    l_proj.wait()
-    for one in h_copies:
-        one.wait_recv()
-    all_heads = jnp.concatenate([h_all[i].astype(F32) for i in range(kv)], axis=0)
-
-    e_all[t_me] = matmul(all_heads.astype(BF16), wproj[...]).astype(BF16)
-    e_copies = [link.copy("tp", p, e_all.at[t_me], e_all.at[t_me]) for p in t_peers]
-    l_gain2.wait()
-    for one in e_copies:
-        one.wait_recv()
-    branch = e_all[0].astype(F32)
-    for i in range(1, tp):
-        branch = branch + e_all[i].astype(F32)
+    loaded(l_proj, wproj.at[0:w_v])
+    remote(wproj.at[0:w_v], wproj.at[0:w_v], w_sent, w_got, {"tp": mate}).wait_recv()
+    n_sent = len(targets)
+    remote(h_all.at[0:n_sent], h_all.at[0:n_sent], h_sent, h_got, near_kv).wait_recv()
+    all_heads = jnp.concatenate(
+        [
+            jnp.concatenate([h_all[c * kv + i].astype(F32) for i in range(kv)], axis=0)
+            for c in range(2)
+        ],
+        axis=1,
+    ).astype(BF16)
+    e_all[t_me] = matmul(all_heads, wproj[...]).astype(BF16)
+    e_sent, e_got = link.phase(), link.slot()
+    for p in t_peers:
+        remote(e_all.at[t_me], e_all.at[t_me], e_sent, e_got, {"tp": p}).start()
+    loaded(l_gain2, gain2)
+    remote(e_all.at[0 : tp - 1], e_all.at[0 : tp - 1], e_sent, e_got, {"tp": mate}).wait_recv()
+    branch = jnp.concatenate(
+        [
+            sum(e_all[i].astype(F32) for i in range(c + 2, tp, 2)) + e_all[c].astype(F32)
+            for c in range(2)
+        ],
+        axis=1,
+    )
     wide_f = jnp.concatenate([tok[i] for i in range(tp)], axis=1).astype(F32)
     middle = (wide_f + branch).astype(BF16).astype(F32)
     for i in range(tp):
         mid[i] = middle[:, i * width : (i + 1) * width]
-    sq_all[k_me] = jnp.broadcast_to(jnp.sum(middle * middle, axis=1, keepdims=True), (rows, 128))
-    s_copies = [link.copy("kv", p, sq_all.at[k_me], sq_all.at[k_me]) for p in k_peers]
+    diagonal = lax.broadcasted_iota(jnp.int32, (rows, 128), 0) == lax.broadcasted_iota(
+        jnp.int32, (rows, 128), 1
+    )
+    row_squares = jnp.sum(middle * middle, axis=1, keepdims=True)
+    sq_all[k_me] = jnp.sum(jnp.where(diagonal, row_squares, 0.0), axis=0, keepdims=True)
+    s_sent, s_got = link.phase(), link.slot()
+    for p in k_peers:
+        remote(sq_all.at[k_me], sq_all.at[k_me], s_sent, s_got, {"kv": p}).start()
     nmid[...] = (middle * gain2[...]).astype(BF16)
 
-    l_up.wait()
-    f_copies = {}
-
-    def raise_block(target, sub, put):
-        first = target * block + sub * half
-
-        def raise_tile(i, carry):
-            cols = pl.ds(pl.multiple_of(first + i * tile, tile), tile)
-            put(pl.ds(pl.multiple_of(i * tile, tile), tile), matmul(nmid[...], wup[:, cols]))
-            return carry
-
-        lax.fori_loop(0, half // tile, raise_tile, 0)
-
+    loaded(l_up, wup)
     is_end = jnp.logical_or(k_me == 0, k_me == kv - 1)
     is_mid = jnp.logical_not(is_end)
     across, skip, near = k_peers
     targets = [across, jnp.where(is_end, near, skip), near]
-    for o in (1, 0, 2):
-        for sub in range(subs):
-
-            def put_sent(here, part, o=o, sub=sub):
-                f_send[o, sub, :, here] = part.astype(BF16)
-
-            raise_block(k_peers[o], sub, put_sent)
-            f_copies[o, sub] = link.copy(
-                "kv",
-                targets[o],
-                f_send.at[o, sub],
-                f_recv.at[o, sub],
-                when=None if o else is_end,
+    place = (0, 2, 1)
+    f_sent = link.phase()
+    f_pair, f_skip = [], []
+    f_across = []
+    for sub in range(subs):
+        pair, alone = link.slot(), link.slot()
+        f_pair.append(pair)
+        f_skip.append(alone)
+        for o in (1, 0, 2):
+            part = matmul(nmid[...], wup[:, columns(k_peers[o] * block + sub * half, half)])
+            f_send[sub, place[o]] = part.astype(BF16)
+        f_own[sub] = matmul(nmid[...], wup[:, columns(k_me * block + sub * half, half)])
+        for o in (1, 0, 2):
+            one = remote(
+                f_send.at[sub, place[o]],
+                f_recv.at[sub, place[o]],
+                f_sent,
+                alone if o == 1 else pair,
+                {"kv": targets[o]},
             )
-    for sub in range(subs):
-        f_copies[1, sub].wait_recv()
-
-        def relay(sub=sub):
-            both = f_send[0, sub].astype(F32) + f_recv[1, sub].astype(F32)
-            f_send[0, sub] = both.astype(BF16)
-            f_copies[0, sub].start()
-
-        pl.when(is_mid)(relay)
-
-        def put_own(here, part, sub=sub):
-            f_own[sub, :, here] = part
-
-        raise_block(k_me, sub, put_own)
-    for one in s_copies:
-        one.wait_recv()
-    row_sum = sq_all[0, :, 0:1]
+            if o:
+                one.start()
+            else:
+                pl.when(is_end)(one.start)
+                f_across.append(one)
+    remote(sq_all.at[0 : kv - 1], sq_all.at[0 : kv - 1], s_sent, s_got, near_kv).wait_recv()
+    row_sum = sq_all[0]
     for i in range(1, kv):
-        row_sum = row_sum + sq_all[i, :, 0:1]
+        row_sum = row_sum + sq_all[i]
+    row_sum = jnp.sum(jnp.where(diagonal, row_sum, 0.0), axis=1, keepdims=True)
     scale_mid = lax.rsqrt(row_sum / total_width + EPSILON)
-    g2_copies = {}
-    for sub in range(subs):
+    g2_sent, g2_got = link.phase(), []
+
+    def relay(sub):
+        here = f_recv.at[sub, 2]
+        remote(here, here, f_sent, f_skip[sub], near_kv).wait_recv()
+
+        def add():
+            both = f_send[sub, 0].astype(F32) + f_recv[sub, 2].astype(F32)
+            f_send[sub, 0] = both.astype(BF16)
+            f_across[sub].start()
+
+        pl.when(is_mid)(add)
+
+    def complete(sub):
+        here = f_recv.at[sub, 0:2]
+        remote(here, here, f_sent, f_pair[sub], near_kv).wait_recv()
         upward = f_own[sub]
-        f_copies[0, sub].wait_recv()
-        f_copies[2, sub].wait_recv()
-        skipped = jnp.where(is_end, f_recv[1, sub].astype(F32), 0.0)
-        upward = upward + f_recv[0, sub].astype(F32) + skipped + f_recv[2, sub].astype(F32)
+        skipped = jnp.where(is_end, f_recv[sub, 2].astype(F32), 0.0)
+        upward = upward + f_recv[sub, 0].astype(F32) + skipped + f_recv[sub, 1].astype(F32)
         hid[k_me, sub] = jnp.square(jnp.maximum(upward * scale_mid, 0.0)).astype(BF16)
         mine = hid.at[k_me, sub]
-        for o, peer in enumerate(k_peers):
-            g2_copies[o, sub] = link.copy("kv", peer, mine, mine)
-
-    for one in l_down:
-        one.wait()
-
-    def lower_block(source, sub, first):
-        deep = pl.ds(pl.multiple_of(source * block + sub * half, half), half)
-        part = matmul(hid[source, sub], wdown[deep, :])
-        down[...] = part if first else down[...] + part
-
+        got = link.slot()
+        g2_got.append(got)
+        for peer in k_peers:
+            remote(mine, mine, g2_sent, got, {"kv": peer}).start()
+
+    ahead = 2
     for sub in range(subs):
-        lower_block(k_me, sub, sub == 0)
+        relay(sub)
+        if sub >= ahead:
+            complete(sub - ahead)
+    for sub in range(subs - min(ahead, subs), subs):
+        complete(sub)
+
+    loaded(l_down, wdown)
+
+    def lower(source, sub):
+        return matmul(hid[source, sub], wdown[columns(source * block + sub * half, half), :])
+
+    part = lower(k_me, 0)
+    for sub in range(1, subs):
+        part = part + lower(k_me, sub)
+    down[...] = part
     for sub in range(subs):
+        here = hid.at[0 : kv - 1, sub]
+        remote(here, here, g2_sent, g2_got[sub], near_kv).wait_recv()
+        part = down[...]
         for o in (2, 1, 0):
-            g2_copies[o, sub].wait_recv()
-            lower_block(k_from[o], sub, False)
+            part = part + lower(k_from[o], sub)
+        down[...] = part
     for i in range(tp):
         d_send[i] = down[:, i * width : (i + 1) * width].astype(BF16)
-    d_copies = [
-        link.copy("tp", p, d_send.at[p], d_recv.at[o]) for o, p in enumerate(t_peers)
-    ]
-    lower = d_send[t_me].astype(F32)
-    for o, one in enumerate(d_copies):
-        one.wait_recv()
-        lower = lower + d_recv[o].astype(F32)
-    out_v[...] = (mid[t_me] + lower).astype(BF16)
-    for one in link.started:
-        one.wait_send()
+    d_sent, d_got = link.phase(), link.slot()
+    for o, p in enumerate(t_peers):
+        remote(d_send.at[p], d_recv.at[o], d_sent, d_got, {"tp": p}).start()
+    own_part = d_send[t_me].astype(F32)
+    remote(d_recv, d_recv, d_sent, d_got, {"tp": mate}).wait_recv()
+    for o in range(tp - 1):
+        own_part = own_part + d_recv[o].astype(F32)
+    out_v[...] = (mid[t_me] + own_part).astype(BF16)
+    for sem, whole in (
+        (a_sent, tok.at[0 : tp - 1]),
+        (w_sent, wproj.at[0:w_v]),
+        (g_sent, g_recv),
+        (b_sent, b_recv),
+        (h_sent, h_all.at[0:n_sent]),
+        (e_sent, e_all.at[0 : tp - 1]),
+        (s_sent, sq_all.at[0 : kv - 1]),
+        (f_sent, f_recv),
+        (g2_sent, hid.at[0 : kv - 1]),
+        (d_sent, d_recv),
+    ):
+        remote(whole, whole, sem, b_got[0], near_kv).wait_send()
 
 
 def finish_kernel(*refs):
@@ -549,44 +618,43 @@
         w_up,
         w_down,
     ))
-    n_copies = count_copies(kv, tp, subs)
+    n_in, n_send, n_recv = semaphore_counts(subs)
+    n_gates = w_input_gate.shape[1]
     vm = pltpu.VMEM
     scratch = [
         vm((tp, rows, width), BF16),
         vm((1, wide), F32),
         vm((wide, n_qkv), BF16),
-        vm(w_input_gate.shape[::-1], BF16),
-        vm(w_forget_gate.shape[::-1], BF16),
-        vm((1, bias_input.shape[0]), F32),
-        vm((1, bias_forget.shape[0]), F32),
+        vm((2 * n_gates, wide), BF16),
+        vm((2, 1, n_gates), F32),
         vm(cell_state.shape, F32),
         vm(norm_state.shape, F32),
         vm(max_state.shape[::-1], F32),
-        vm(w_proj.shape, BF16),
+        vm((2 * w_v, wide // 2), BF16),
         vm((1, wide), F32),
         vm(w_up.shape, BF16),
         vm(w_down.shape, BF16),
         vm((kv, own_rows, n_qkv), F32),
         vm((kv, own_rows, n_qkv), BF16),
         vm((kv - 1, own_rows, n_qkv), BF16),
-        vm((kv, own_rows, 384), F32),
-        vm((kv - 1, own_rows, 384), F32),
+        vm((kv, own_rows, 128), F32),
+        vm((kv - 1, own_rows, 128), F32),
         vm((own_rows, w_v), F32),
-        vm((kv, own_rows, w_v), BF16),
-        vm((tp, rows, wide), BF16),
-        vm((kv, rows, 128), F32),
+        vm((2 * kv, own_rows, w_v), BF16),
+        vm((tp, rows, wide // 2), BF16),
+        vm((kv, 1, 128), F32),
         vm((tp, rows, width), F32),
         vm((rows, wide), BF16),
         vm((subs, rows, half), F32),
-        vm((kv - 1, subs, rows, half), BF16),
-        vm((kv - 1, subs, rows, half), BF16),
+        vm((subs, kv - 1, rows, half), BF16),
+        vm((subs, kv - 1, rows, half), BF16),
         vm((kv, subs, rows, half), BF16),
         vm((rows, wide), F32),
         vm((tp, rows, width), BF16),
         vm((tp - 1, rows, width), BF16),
-        pltpu.SemaphoreType.DMA((16 + kv,)),
-        pltpu.SemaphoreType.DMA((n_copies,)),
-        pltpu.SemaphoreType.DMA((n_copies,)),
+        pltpu.SemaphoreType.DMA((n_in,)),
+        pltpu.SemaphoreType.DMA((n_send,)),
+        pltpu.SemaphoreType.DMA((n_recv,)),
     ]
     anywhere = pl.BlockSpec(memory_space=pltpu.HBM)
     in_vmem = pl.BlockSpec(memory_space=pltpu.VMEM)
@@ -620,7 +688,7 @@
     tokens, w_query, cell_state, w_up = args[0], args[2], args[10], args[15]
     return (
         kv == 4
-        and tp > 1
+        and tp == 4
         and tokens.shape[1] % 128 == 0
         and w_query.shape[0] % 256 == 0
         and w_query.shape[1] % 256 == 0
@@ -629,7 +697,9 @@
         and 2 * cell_state.shape[0] <= 128
         and cell_state.shape[3] % 128 == 0
         and w_up.shape[1] % (512 * kv) == 0
-        and args[6].shape[1] <= 128
+        and args[6].shape[1] % 16 == 0
+        and 2 * args[6].shape[1] < 128
+        and tokens.shape[0] <= 128
     )
 
 

time: 41.6 us -> 41.1 us (0.988)
    pallas_call x1, Pallas kernels: 39.7 us -> 39.2 us  [fused_on_device(): pl.pallas_call(functools.partial(layer_kernel, kv, tp, subs), out_shape=(...]
where the time goes in v1:
time: 41.1 us; the launch traced here: 40.9 us
  Pallas kernels  40.3 us (98%)
  between operations  0.65 us (2%)
    pallas_call x1, Pallas kernels, fused_on_device(): pl.pallas_call(functools.partial(layer_kernel, kv, tp, subs), out_shape=(...  39.2 us
    pallas_call x1, Pallas kernels, fused_on_device(): pl.pallas_call(finish_kernel, out_shape=tuple((jax.ShapeDtypeStruct(one.s...  1.02 us

profile of v1, /device:TPU:0, one launch (start us, length us, event | category | flops | bytes accessed | tf_op | source)
XLA Modules:
  0.0 40.9 jit_solution(3370094722103596085)
XLA Ops:
  0.6 39.2 %shard_map.192 = (bf16[32,256]{1,0:T(8,128)(2,1)S(1)}, f32[8,4,64,128]{3,2,1,0:T(8,128)S(1)}, f32[8,4,64]{2,1,0:T(4,128)S(1)}, f32[4,8]{1,0:T(4,128)S(1)}) custom-call(bf16[32,256]{1,0:T(8,128)(2,1)} %tokens.1, f32[1,1024]{1,0:T(1,128)} %bitcast.10, bf16[1024,256]{1,0:T(8,128)(2,1)} %w_query.1, bf16[1024,256]{1,0:T(8,128)(2,1)} %w_key.1, ...), custom_call_target="tpu_custom_call" | custom-call | tf_op jit(solution)/shard_map/pallas_call | solution.py:661
  39.9 1.0 %shard_map.193 = (bf16[32,256]{1,0:T(8,128)(2,1)}, f32[8,4,64,128]{3,2,1,0:T(8,128)}, f32[8,4,64]{2,1,0:T(4,128)}, f32[4,8]{1,0:T(4,128)}) custom-call(bf16[32,256]{1,0:T(8,128)(2,1)S(1)} %get-tuple-element.12.refs_0_, f32[8,4,64,128]{3,2,1,0:T(8,128)S(1)} %get-tuple-element.13.refs_1_, f32[8,4,64]{2,1,0:T(4,128)S(1)} %get-tuple-element.14.refs_2_, ...), custom_call_target="tpu_custom_call" | custom-call | tf_op jit(solution)/shard_map/pallas_call | solution.py:676
